TPU v7x, 32 devices: a whole 2x2x4 slice. The times are simulated.
32 devices in a mesh: fs: 4 (over y, x), tp: 8 (over z, core).
Axes of the slice: x: 2, y: 2, z: 4, core: 2. Of those that a mesh axis runs over, the one named last changes fastest.
Arguments:
- tokens: bfloat16 [2048, 2048], P('fs', 'tp'), may hold values from -6 to 6
- norm_gain: float32 [2048], P('fs'), may hold values from 0.1 to 1.9
- gate_train: float32 [2048, 8192], P('fs', 'tp'), may hold values from -0.125 to 0.125
- up_train: float32 [2048, 8192], P('fs', 'tp'), may hold values from -0.125 to 0.125
- down_train: float32 [8192, 2048], P('fs', 'tp'), may hold values from -0.0625 to 0.0625
Outputs:
- gate_serve: bfloat16 [2048, 8192], P(None, 'tp')
- up_serve: bfloat16 [2048, 8192], P(None, 'tp')
- down_serve: bfloat16 [8192, 2048], P('tp')
- layer_out: bfloat16 [2048, 2048], P(('fs', 'tp'))
All inputs are finite; a program needn't handle non-finite values.
Results may differ from a plain program's by a relative error of at most 0.024.
Values may be sent and summed in bfloat16 or wider, within the bound.
A program may use at most 64 MiB of HBM per device.

v0:
```python
import jax
import jax.numpy as jnp
from jax import lax
from jax.sharding import PartitionSpec as P

D = 2048


epsilon = 1e-06


def body(tokens, norm_gain, gate_train, up_train, down_train):
    gate_local = (norm_gain[:, None] * gate_train).astype(jnp.bfloat16)
    up_local = (norm_gain[:, None] * up_train).astype(jnp.bfloat16)
    down_local = down_train.astype(jnp.bfloat16)
    features = lax.all_gather(tokens, "tp", axis=1, tiled=True)
    wide = features.astype(jnp.float32)
    squares = jnp.sum(wide * wide, axis=1)
    gate_whole, up_whole = (
        lax.all_gather(gate_local, "fs", axis=0, tiled=True),
        lax.all_gather(up_local, "fs", axis=0, tiled=True),
    )
    gate_sum = jnp.dot(features, gate_whole, preferred_element_type=jnp.float32)
    up_sum = jnp.dot(features, up_whole, preferred_element_type=jnp.float32)
    down_rows = lax.all_gather(down_local, "fs", axis=0, tiled=True)
    down_whole = lax.all_to_all(down_rows, "tp", split_axis=0, concat_axis=1, tiled=True)
    scale = lax.rsqrt(squares / D + epsilon)[:, None]
    hidden = (jax.nn.silu(gate_sum * scale) * (up_sum * scale)).astype(jnp.bfloat16)
    mixed = lax.psum_scatter(
        jnp.dot(hidden, down_whole, preferred_element_type=jnp.float32).astype(jnp.bfloat16),
        "tp",
        scatter_dimension=0,
        tiled=True,
    )
    return (gate_whole, up_whole, down_whole, mixed)


def solution(mesh):
    return jax.shard_map(
        body,
        mesh=mesh,
        in_specs=(P("fs", "tp"), P("fs"), P("fs", "tp"), P("fs", "tp"), P("fs", "tp")),
        out_specs=(P(None, "tp"), P(None, "tp"), P("tp", None), P(("fs", "tp"), None)),
        check_vma=False,
    )
```

profile of v0, /device:TPU:0, one launch (start us, length us, event | category | flops | bytes accessed | tf_op | source)
XLA Modules:
  0.0 293.7 jit_solution(2137613969868247611)
XLA Ops:
  7.2 0.0 copy-start.2
  7.2 0.0 copy-start.3
  7.2 0.0 all-gather.9.cloned.1.call-start
  7.2 2.8 convert_element_type.20
  10.0 0.0 all-gather.9.cloned.1.call-update
  10.1 0.0 all-gather.11.cloned.1.call-start
  10.1 0.7 all-gather.11.cloned.1.call-update
  10.8 0.0 all-gather.5.cloned.1.call-start
  10.9 0.0 copy-done.2
  10.9 0.0 copy-done.3
  10.9 3.2 %multiply_convert_fusion = (bf16[512,1024]{1,0:T(8,128)(2,1)}, bf16[512,1024]{1,0:T(8,128)(2,1)}) fusion(f32[512,1024]{1,0:T(8,128)S(1)} %copy-done.2, f32[512]{0:T(512)S(1)} %copy-done.3, f32[512,1024]{1,0:T(8,128)} %param.7), kind=kLoop, calls=%fused_computation.9 | loop fusion | flops 2097152 | bytes 6293504 | tf_op jit(solution)/shard_map/convert_element_type | solution.py:14
  14.1 0.0 all-gather.5.cloned.1.call-update
  14.1 51.6 %all-gather.9.cloned.1.call-done = bf16[8192,256]{1,0:T(8,128)(2,1)} async-done(((bf16[2048,256]{1,0:T(8,128)(2,1)}), bf16[8192,256]{1,0:T(8,128)(2,1)}) %all-gather.9.cloned.1.call-update) | async-done | bytes 4194320 | tf_op jit(solution)/shard_map/all_gather | solution.py:25
  65.7 4.6 %all-to-all-start = ((bf16[8,1024,256]{2,1,0:T(8,128)(2,1)}), bf16[8,1024,256]{2,1,0:T(8,128)(2,1)}, u32[]{:S(2)}, u32[]{:S(2)}) async-start(bf16[8,1024,256]{2,1,0:T(8,128)(2,1)} %bitcast.32), calls=%async_computation | async-start | bytes 8388608 | tf_op jit(solution)/shard_map/all_to_all | solution.py:26
  70.3 0.0 all-gather.7.cloned.1.call-start
  70.4 0.5 all-gather.7.cloned.1.call-update
  70.9 0.0 reduce-scatter.2.cloned.1.call-start
  71.0 50.9 %all-gather.11.cloned.1.call-done = bf16[512,2048]{1,0:T(8,128)(2,1)} async-done(((bf16[512,256]{1,0:T(8,128)(2,1)}), bf16[512,2048]{1,0:T(8,128)(2,1)}) %all-gather.11.cloned.1.call-update) | async-done | bytes 2097168 | tf_op jit(solution)/shard_map/all_gather | solution.py:16
  121.8 2.2 multiply_reduce_fusion
  124.1 54.8 %all-gather.5.cloned.1.call-done = bf16[2048,1024]{1,0:T(8,128)(2,1)} async-done(((bf16[512,1024]{1,0:T(8,128)(2,1)}), bf16[2048,1024]{1,0:T(8,128)(2,1)}) %all-gather.5.cloned.1.call-update) | async-done | bytes 4194320 | tf_op jit(solution)/shard_map/all_gather | solution.py:20
  178.9 0.0 copy-done.1
  178.9 5.9 %fusion.5 = f32[1024,512]{1,0:T(8,128)} fusion(bf16[2048,1024]{1,0:T(8,128)(2,1)} %all-gather.5.cloned.1.call-done, bf16[512,2048]{1,0:T(8,128)(2,1)S(1)} %copy-done.1), kind=kOutput, calls=%fused_computation.13 | convolution fusion | flops 2147483648 | bytes 8388608 | tf_op jit(solution)/shard_map/dot_general | solution.py:23
  184.8 0.0 all-to-all-done
  184.8 6.5 %copy.10 = bf16[8,1024,256]{1,2,0:T(8,128)(2,1)} copy(bf16[8,1024,256]{2,1,0:T(8,128)(2,1)} %all-to-all-done) | data formatting | bytes 8388608 | tf_op jit(solution)/shard_map/all_to_all | solution.py:26
  191.2 42.5 %all-gather.7.cloned.1.call-done = bf16[2048,1024]{1,0:T(8,128)(2,1)} async-done(((bf16[512,1024]{1,0:T(8,128)(2,1)}), bf16[2048,1024]{1,0:T(8,128)(2,1)}) %all-gather.7.cloned.1.call-update) | async-done | bytes 4194320 | tf_op jit(solution)/shard_map/all_gather | solution.py:21
  233.7 10.3 %convolution_convert_fusion = bf16[512,2048]{1,0:T(8,128)(2,1)} fusion(bf16[1024,2048]{0,1:T(8,128)(2,1)} %bitcast.30, f32[1024,512]{1,0:T(8,128)} %fusion.5, bf16[2048,1024]{1,0:T(8,128)(2,1)} %all-gather.7.cloned.1.call-done, bf16[512,2048]{1,0:T(8,128)(2,1)S(1)} %copy-done.1, f32[512]{0:T(512)S(1)} %add_rsqrt_fusion), kind=kOutput, calls=%fused_computation.1 | convolution fusion | flops 4300210176 | bytes 14682112 | tf_op jit(solution)/shard_map/dot_general | solution.py:30
  244.0 0.0 reduce-scatter.2.cloned.1.call-update
  244.0 6.4 %copy.11 = bf16[1024,2048]{1,0:T(8,128)(2,1)} copy(bf16[1024,2048]{0,1:T(8,128)(2,1)} %bitcast.31) | data formatting | bytes 8388608
  250.5 29.8 %reduce-scatter.2.cloned.1.call-done = bf16[64,2048]{1,0:T(8,128)(2,1)} async-done(((bf16[512,2048]{1,0:T(8,128)(2,1)}), bf16[64,2048]{1,0:T(8,128)(2,1)}) %reduce-scatter.2.cloned.1.call-update) | async-done | bytes 262160 | tf_op jit(solution)/shard_map/reduce_scatter | solution.py:29
  280.3 4.8 %copy.14 = bf16[2048,1024]{1,0:T(8,128)(2,1)} copy(bf16[2048,1024]{1,0:T(8,128)(2,1)} %all-gather.5.cloned.1.call-done) | data formatting | bytes 8388608
  285.1 0.0 copy-done
  285.1 2.0 copy.15
  (3 shorter events, 0.0 us)
Async XLA Ops:
  7.2 3.7 %copy-start.2 = (f32[512,1024]{1,0:T(8,128)S(1)}, f32[512,1024]{1,0:T(8,128)}, u32[]{:S(2)}) copy-start(f32[512,1024]{1,0:T(8,128)} %param.8) | copy-start | bytes 6291460
  7.2 3.7 %copy-start.3 = (f32[512]{0:T(512)S(1)}, f32[512]{0:T(512)}, u32[]{:S(2)}) copy-start(f32[512]{0:T(512)} %param.6) | copy-start | bytes 6148
  7.2 58.6 %all-gather.9.cloned.1.call-start = ((), (), s32[]{:S(2)}) async-start(), calls=%async_computation.4 | async-start | bytes 5242880 | tf_op jit(solution)/shard_map/all_gather | solution.py:25
  10.1 111.8 %all-gather.11.cloned.1.call-start = ((), (), s32[]{:S(2)}) async-start(), calls=%async_computation.5 | async-start | bytes 2359296 | tf_op jit(solution)/shard_map/all_gather | solution.py:16
  10.8 168.1 %all-gather.5.cloned.1.call-start = ((), (), s32[]{:S(2)}) async-start(), calls=%async_computation.2 | async-start | bytes 5242880 | tf_op jit(solution)/shard_map/all_gather | solution.py:20
  65.7 119.0 %all-to-all-start = ((bf16[8,1024,256]{2,1,0:T(8,128)(2,1)}), bf16[8,1024,256]{2,1,0:T(8,128)(2,1)}, u32[]{:S(2)}, u32[]{:S(2)}) async-start(bf16[8,1024,256]{2,1,0:T(8,128)(2,1)} %bitcast.32), calls=%async_computation | async-start | bytes 8388608 | tf_op jit(solution)/shard_map/all_to_all | solution.py:26
  70.3 163.4 %all-gather.7.cloned.1.call-start = ((), (), s32[]{:S(2)}) async-start(), calls=%async_computation.3 | async-start | bytes 5242880 | tf_op jit(solution)/shard_map/all_gather | solution.py:21
  70.9 209.4 %reduce-scatter.2.cloned.1.call-start = ((), (), s32[]{:S(2)}) async-start(), calls=%async_computation.6 | async-start | bytes 2359296 | tf_op jit(solution)/shard_map/reduce_scatter | solution.py:29
  121.8 57.0 %copy-start.1 = (bf16[512,2048]{1,0:T(8,128)(2,1)S(1)}, bf16[512,2048]{1,0:T(8,128)(2,1)}, u32[]{:S(2)}) copy-start(bf16[512,2048]{1,0:T(8,128)(2,1)} %all-gather.11.cloned.1.call-done) | copy-start | bytes 6291460
  280.3 4.8 %copy-start = (bf16[2048,1024]{1,0:T(8,128)(2,1)S(1)}, bf16[2048,1024]{1,0:T(8,128)(2,1)}, u32[]{:S(2)}) copy-start(bf16[2048,1024]{1,0:T(8,128)(2,1)} %all-gather.7.cloned.1.call-done) | copy-start | bytes 12582916
Sparse Core Ops, SparseCore 0:
  10.4 55.2 all-gather.8
  67.3 54.4 all-gather.10
  124.3 54.5 all-gather.4
  181.1 52.5 all-gather.6
  244.2 36.0 reduce-scatter.1
where the time goes:
time: 294 us
  waiting for transfers between devices  231 us (79%)
  local copies, waits for them, and re-layouts  19.8 us (7%)
  matrix products  16.2 us (6%)
  between operations  13.8 us (5%)
  other arithmetic  8.23 us (3%)
  starting transfers between devices  4.8 us (2%)
    all_gather x1, waiting for transfers between devices, body(): lax.all_gather(gate_local, 'fs', axis=0, tiled=True)  54.8 us
    all_gather x1, waiting for transfers between devices, body(): down_rows = lax.all_gather(down_local, 'fs', axis=0, tiled=True)  51.6 us
    all_gather x1, waiting for transfers between devices, body(): features = lax.all_gather(tokens, 'tp', axis=1, tiled=True)  50.9 us
    all_gather x1, waiting for transfers between devices, body(): lax.all_gather(up_local, 'fs', axis=0, tiled=True)  42.5 us
    reduce_scatter x1, waiting for transfers between devices, body(): lax.psum_scatter(jnp.dot(hidden, down_whole, preferred_element_type=jnp.f...  29.8 us
    unnamed x11, local copies, waits for them, and re-layouts  13.3 us
    dot_general x1, matrix products, body(): jnp.dot(hidden, down_whole, preferred_element_type=jnp.float32)  10.3 us
    all_to_all x1, local copies, waits for them, and re-layouts, body(): lax.all_to_all(down_rows, 'tp', split_axis=0, concat_axis=1, tiled=True)  6.48 us
  transfers between devices with their start and end apart: 6, of which 5 were waited for; matrix products, arithmetic and copies ran while one was open for 8% of the time, Pallas kernels for 0%

commit v1 on v0

v1 whole, which is shorter than its diff:
```python
import functools

import jax
import jax.numpy as jnp
from jax import lax
from jax.experimental import pallas as pl
from jax.experimental.pallas import tpu as pltpu
from jax.sharding import PartitionSpec as P

MESH = pl.DeviceIdType.MESH
BF16 = jnp.bfloat16
F32 = jnp.float32
epsilon = 1e-06
CHUNKS = 4
X_ORDER = (0, 1, 2, 3)
Y_ORDER = (2, 3, 0, 1)


def flip(a, k):
    result = 0
    for bit in (1, 2, 4):
        own, other = (a // bit) % 2, (k // bit) % 2
        result = result + bit * (own + other - 2 * own * other)
    return result


def kernel(
    tok_in, gain_in, gate_in, up_in, down_in,
    gate_out, up_out, down_out, layer_out,
    w32, d32, wbuf, dcast, dbuf, tbuf, acc, hidden, scale, keep, psend, precv, zsend, zrecv,
    load_w, load_d, tok_s, tok_r, own_s, fwd_s, w_r, dz_s, d_s, d_r, out_w, out_d, p_s, p_r, z_s, z_r,
):
    f, t = lax.axis_index("fs"), lax.axis_index("tp")
    n_tp, n_fs = tbuf.shape[0], wbuf.shape[1]
    z, core = t // 2, t % 2
    fx, fy, fd = flip(f, 1), flip(f, 2), flip(f, 3)
    mate = flip(t, 1)
    rows = wbuf.shape[2]
    part = rows // CHUNKS
    w_ins, w_outs = (gate_in, up_in), (gate_out, up_out)
    tall, width = dbuf.shape[1], dbuf.shape[2]
    half = tall // 2
    per = n_tp // n_fs
    n_tok = tbuf.shape[1]
    piece_rows = n_tok // n_tp

    def remote(src, dst, ss, rs, to_f, to_t):
        return pltpu.make_async_remote_copy(
            src_ref=src, dst_ref=dst, send_sem=ss, recv_sem=rs, device_id=(to_f, to_t), device_id_type=MESH
        )

    def load(w, i):
        return pltpu.make_async_copy(w_ins[w].at[pl.ds(i * part, part)], w32.at[w, pl.ds(i * part, part)], load_w.at[w, i])

    order = (0, 2, 1, 3)
    for i in order:
        for w in range(2):
            load(w, i).start()
    load_down = [
        pltpu.make_async_copy(down_in.at[pl.ds(c * tall, tall)], d32.at[pl.ds(c * tall, tall)], load_d.at[c])
        for c in range(per)
    ]
    for copy in load_down:
        copy.start()

    barrier = pltpu.get_barrier_semaphore()
    peers = [(fx, t), (fy, t)] + [(f, flip(t, k)) for k in range(1, n_tp)]
    for peer in peers:
        pl.semaphore_signal(barrier, inc=1, device_id=peer, device_id_type=MESH)

    tbuf[t] = tok_in[...]

    def cast(w, i):
        block = pl.ds(i * part, part)
        load(w, i).wait()
        wbuf[w, f, block] = (gain_in[block] * w32[w, block]).astype(BF16)

    for i in order:
        for w in range(2):
            cast(w, i)
    pl.semaphore_wait(barrier, len(peers))

    def tok_copy(src, piece, slot, to):
        return remote(src, tbuf.at[piece], tok_s.at[slot], tok_r.at[piece], f, to)

    for slot, k in enumerate((1, 2, 4, 6)):
        tok_copy(tok_in, t, slot, flip(t, k)).start()

    def w_copy(w, src, i, sem, to):
        ref = wbuf.at[w, src, pl.ds(i * part, part)]
        return remote(ref, ref, sem, w_r.at[w, src, i], to, t)

    for step in range(CHUNKS):
        for w in range(2):
            w_copy(w, f, X_ORDER[step], own_s.at[0, w, X_ORDER[step]], fx).start()
            w_copy(w, f, Y_ORDER[step], own_s.at[1, w, Y_ORDER[step]], fy).start()

    def dz_copy(c, h):
        block = pl.ds(h * half, half)
        return remote(dcast.at[c, block], dbuf.at[t, block], dz_s.at[c, h], d_r.at[t, h], f, f * per + c)

    for c in range(per):
        load_down[c].wait()
        for h in range(2):
            block = pl.ds(h * half, half)
            dcast[c, block] = d32[pl.ds(c * tall + h * half, half)].astype(BF16)

        @pl.when(t == f * per + c)
        def _():
            dbuf[t] = dcast[c]

    for h in range(2):
        for c in range(per):
            @pl.when(t != f * per + c)
            def _():
                dz_copy(c, h).start()

    def store_w(w, src):
        return pltpu.make_async_copy(wbuf.at[w, src], w_outs[w].at[pl.ds(src * rows, rows)], out_w.at[w, src])

    for w in range(2):
        store_w(w, f).start()

    def arrive(step, w):
        i = X_ORDER[step]
        w_copy(w, fx, i, fwd_s.at[w, i], fy).wait_recv()
        if i < CHUNKS // 2:
            w_copy(w, fx, i, fwd_s.at[w, i], fy).start()
        i = Y_ORDER[step]
        w_copy(w, fy, i, fwd_s.at[w, i], fx).wait_recv()
        if i >= CHUNKS // 2:
            w_copy(w, fy, i, fwd_s.at[w, i], fx).start()

    tile = 256

    def accumulate(src, first):
        def one(n, _):
            w, column = n // (wbuf.shape[3] // tile), pl.multiple_of(n % (wbuf.shape[3] // tile) * tile, tile)
            total = 0.0 if first else acc[w, :, pl.ds(column, tile)]
            for p in range(per):
                total = total + jnp.dot(
                    tbuf[src * per + p],
                    wbuf[w, src, pl.ds(p * width, width), pl.ds(column, tile)],
                    preferred_element_type=F32,
                )
            acc[w, :, pl.ds(column, tile)] = total
            return 0

        lax.fori_loop(0, 2 * (wbuf.shape[3] // tile), one, 0)

    for step in range(CHUNKS // 2):
        for w in range(2):
            arrive(step, w)
    for slot, k in enumerate((2, 4, 6)):
        piece = flip(t, k)
        tok_copy(tok_in, piece, 4 + slot, mate).wait_recv()
        tok_copy(tbuf.at[piece], piece, 4 + slot, mate).start()
    for k in (1, 3, 5, 7):
        tok_copy(tok_in, flip(t, k), 0, mate).wait_recv()
    squares = jnp.zeros((n_tok, 1), F32)
    for p in range(n_tp):
        wide = tbuf[p].astype(F32)
        squares = squares + jnp.sum(wide * wide, axis=1, keepdims=True)
    scale[...] = lax.rsqrt(squares / (n_tp * width) + epsilon)
    accumulate(f, True)
    for step in range(CHUNKS // 2, CHUNKS):
        for w in range(2):
            arrive(step, w)
    for src in (fx, fy):
        for w in range(2):
            store_w(w, src).start()

    owner = t // per
    low, high = (f % 2 + owner % 2) % 2, (f // 2 + owner // 2) % 2
    is_source = f == owner
    to_first = fx + (fy - fx) * (low * (1 - high))
    to_second = fy + (fx - fy) * ((1 - low) * high)
    ends = ((1 - low) * high, low * (1 - high))
    nexts = (to_first, to_second)

    def d_copy(piece, h):
        ref = dbuf.at[piece, pl.ds(h * half, half)]
        return remote(ref, ref, d_s.at[piece, h], d_r.at[piece, h], nexts[h], t)

    def take(k):
        piece = flip(t, k)
        for h in range(2):
            @pl.when(jnp.logical_or(jnp.logical_not(is_source), k != 0))
            def _():
                d_copy(piece, h).wait_recv()

            @pl.when(ends[h] == 0)
            def _():
                d_copy(piece, h).start()

    @pl.when(is_source)
    def _():
        take(0)
        take(1)

    accumulate(fx, False)
    accumulate(fy, False)
    for i in (0, 2, 1, 3):
        for w in range(2):
            w_copy(w, fd, i, fwd_s.at[w, i], fx).wait_recv()
    for w in range(2):
        store_w(w, fd).start()
    accumulate(fd, False)

    def make_hidden(n, _):
        columns = pl.ds(pl.multiple_of(n * tile, tile), tile)
        s = scale[...]
        g = acc[0, :, columns] * s
        hidden[:, columns] = (g / (1.0 + jnp.exp(-g)) * (acc[1, :, columns] * s)).astype(BF16)
        return 0

    lax.fori_loop(0, hidden.shape[1] // tile, make_hidden, 0)

    def store_d(piece):
        columns = pl.ds(pl.multiple_of(piece * width, width), width)
        return pltpu.make_async_copy(dbuf.at[piece], down_out.at[:, columns], out_d.at[piece])

    def p_copy(k):
        return remote(psend.at[k], precv.at[k], p_s.at[k], p_r.at[k], f, mate)

    def z_copy(k, dz, piece):
        to = flip(t, 2 * dz)
        return remote(zsend.at[k, to // 2], zrecv.at[z, piece], z_s.at[k, dz], z_r.at[z, piece], f, to)

    def z_arrival(dz, piece):
        src = flip(t, 2 * dz)
        return remote(zsend.at[0, 0], zrecv.at[src // 2, piece], z_s.at[0, dz], z_r.at[src // 2, piece], f, src)

    n_z = n_tp // 2

    def finish(k):
        p_copy(k).wait_recv()
        for b in range(n_z):
            block = (keep[flip(k, 1), b] + precv[k, b].astype(F32)).astype(BF16)
            zsend[k, b] = block
        piece = flip(mate, k)
        zrecv[z, piece] = zsend[k, z]
        for dz in range(1, n_z):
            z_copy(k, dz, piece).start()

    def product(k):
        piece = flip(t, k)
        store_d(piece).start()
        out = jnp.dot(hidden[...], dbuf[piece], preferred_element_type=F32)
        out = out.reshape(n_z, 2, piece_rows, width)

        @pl.when(core == 0)
        def _():
            keep[k] = out[:, 0]
            psend[k] = out[:, 1].astype(BF16)

        @pl.when(core == 1)
        def _():
            keep[k] = out[:, 1]
            psend[k] = out[:, 0].astype(BF16)

        p_copy(k).start()

    def pair(i, _):
        for c in range(2):
            k = 2 * i + c

            @pl.when(jnp.logical_not(jnp.logical_and(is_source, i == 0)))
            def _():
                take(k)

            product(k)
        for c in range(2):
            finish(2 * i + c)
        return 0

    lax.fori_loop(0, n_tp // 2, pair, 0)

    for k in range(n_tp):
        for dz in range(1, n_z):
            z_arrival(dz, k).wait_recv()
    for piece in range(n_tp):
        total = zrecv[0, piece].astype(F32)
        for b in range(1, n_z):
            total = total + zrecv[b, piece].astype(F32)
        layer_out[:, pl.ds(piece * width, width)] = total.astype(BF16)

    for slot in range(4):
        tok_copy(tok_in, t, slot, mate).wait_send()
    for slot in range(3):
        tok_copy(tok_in, t, 4 + slot, mate).wait_send()
    for w in range(2):
        for i in range(CHUNKS):
            w_copy(w, f, i, own_s.at[0, w, i], fx).wait_send()
            w_copy(w, f, i, own_s.at[1, w, i], fy).wait_send()
            w_copy(w, f, i, fwd_s.at[w, i], fx).wait_send()
        for src in range(n_fs):
            store_w(w, src).wait()
    for c in range(per):
        for h in range(2):
            @pl.when(t != f * per + c)
            def _():
                dz_copy(c, h).wait_send()
    for k in range(n_tp):
        store_d(k).wait()
        p_copy(k).wait_send()
        for dz in range(1, n_z):
            z_copy(k, dz, k).wait_send()
        for h in range(2):
            @pl.when(ends[h] == 0)
            def _():
                d_copy(k, h).wait_send()


def body(tokens, norm_gain, gate_train, up_train, down_train, *, n_fs, n_tp):
    n_tok, width = tokens.shape
    rows, cols = gate_train.shape
    tall = down_train.shape[0] * n_fs // n_tp
    piece_rows = n_tok // n_tp
    n_z = n_tp // 2
    hbm = pl.BlockSpec(memory_space=pl.ANY)
    vmem = pl.BlockSpec(memory_space=pltpu.VMEM)
    dma = pltpu.SemaphoreType.DMA
    return pl.pallas_call(
        kernel,
        out_shape=(
            jax.ShapeDtypeStruct((rows * n_fs, cols), BF16),
            jax.ShapeDtypeStruct((rows * n_fs, cols), BF16),
            jax.ShapeDtypeStruct((tall, width * n_tp), BF16),
            jax.ShapeDtypeStruct((piece_rows, width * n_tp), BF16),
        ),
        in_specs=[vmem, vmem, hbm, hbm, hbm],
        out_specs=(hbm, hbm, hbm, vmem),
        scratch_shapes=[
            pltpu.VMEM((2, rows, cols), F32),
            pltpu.VMEM(down_train.shape, F32),
            pltpu.VMEM((2, n_fs, rows, cols), BF16),
            pltpu.VMEM((n_tp // n_fs, tall, width), BF16),
            pltpu.VMEM((n_tp, tall, width), BF16),
            pltpu.VMEM((n_tp, n_tok, width), BF16),
            pltpu.VMEM((2, n_tok, cols), F32),
            pltpu.VMEM((n_tok, cols), BF16),
            pltpu.VMEM((n_tok, 1), F32),
            pltpu.VMEM((n_tp, n_z, piece_rows, width), F32),
            pltpu.VMEM((n_tp, n_z, piece_rows, width), BF16),
            pltpu.VMEM((n_tp, n_z, piece_rows, width), BF16),
            pltpu.VMEM((n_tp, n_z, piece_rows, width), BF16),
            pltpu.VMEM((n_z, n_tp, piece_rows, width), BF16),
            dma((2, CHUNKS)),
            dma((n_tp // n_fs,)),
            dma((7,)),
            dma((n_tp,)),
            dma((2, 2, CHUNKS)),
            dma((2, CHUNKS)),
            dma((2, n_fs, CHUNKS)),
            dma((n_tp // n_fs, 2)),
            dma((n_tp, 2)),
            dma((n_tp, 2)),
            dma((2, n_fs)),
            dma((n_tp,)),
            dma((n_tp,)),
            dma((n_tp,)),
            dma((n_tp, n_z)),
            dma((n_z, n_tp)),
        ],
        compiler_params=pltpu.CompilerParams(
            collective_id=0, has_side_effects=True, vmem_limit_bytes=60 * 1024 * 1024
        ),
    )(tokens, norm_gain[:, None], gate_train, up_train, down_train)


def plain(tokens, norm_gain, gate_train, up_train, down_train):
    gate_local = (norm_gain[:, None] * gate_train).astype(BF16)
    up_local = (norm_gain[:, None] * up_train).astype(BF16)
    down_local = down_train.astype(BF16)
    features = lax.all_gather(tokens, "tp", axis=1, tiled=True)
    wide = features.astype(F32)
    squares = jnp.sum(wide * wide, axis=1)
    gate_whole = lax.all_gather(gate_local, "fs", axis=0, tiled=True)
    up_whole = lax.all_gather(up_local, "fs", axis=0, tiled=True)
    gate_sum = jnp.dot(features, gate_whole, preferred_element_type=F32)
    up_sum = jnp.dot(features, up_whole, preferred_element_type=F32)
    down_rows = lax.all_gather(down_local, "fs", axis=0, tiled=True)
    down_whole = lax.all_to_all(down_rows, "tp", split_axis=0, concat_axis=1, tiled=True)
    scale = lax.rsqrt(squares / features.shape[1] + epsilon)[:, None]
    hidden = (jax.nn.silu(gate_sum * scale) * (up_sum * scale)).astype(BF16)
    mixed = lax.psum_scatter(
        jnp.dot(hidden, down_whole, preferred_element_type=F32).astype(BF16), "tp", scatter_dimension=0, tiled=True
    )
    return (gate_whole, up_whole, down_whole, mixed)


def solution(mesh):
    n_fs, n_tp = mesh.shape["fs"], mesh.shape["tp"]
    fast = n_fs == 4 and n_tp == 8
    return jax.shard_map(
        functools.partial(body, n_fs=n_fs, n_tp=n_tp) if fast else plain,
        mesh=mesh,
        in_specs=(P("fs", "tp"), P("fs"), P("fs", "tp"), P("fs", "tp"), P("fs", "tp")),
        out_specs=(P(None, "tp"), P(None, "tp"), P("tp", None), P(("fs", "tp"), None)),
        check_vma=False,
    )
```

time: 294 us -> 310 us (1.054)
  Pallas kernels: 0 us -> 295 us
  waiting for transfers between devices: 231 us -> 0 us
  matrix products: 16.2 us -> 0 us
  between operations: 13.8 us -> 0.65 us
  other arithmetic: 8.23 us -> 0 us
  local copies, waits for them, and re-layouts: 19.8 us -> 12.8 us
  starting transfers between devices: 4.8 us -> 0 us
    pallas_call x0 -> x1, Pallas kernels: none -> 295 us  [body(): pl.pallas_call(kernel, out_shape=(jax.ShapeDtypeStruct((rows * n_fs, cols...]
    all_gather x4 -> x0, waiting for transfers between devices: 200 us -> none  [the longest x1 54.8 us: body(): lax.all_gather(gate_local, 'fs', axis=0, tiled=True)]
    reduce_scatter x1 -> x0, waiting for transfers between devices: 29.8 us -> none  [body(): lax.psum_scatter(jnp.dot(hidden, down_whole, preferred_element_type=jnp.f...]
    dot_general x2 -> x0, matrix products: 16.2 us -> none  [the longest x1 10.3 us: body(): jnp.dot(hidden, down_whole, preferred_element_type=jnp.float32)]
    all_to_all x1 -> x0, local copies, waits for them, and re-layouts: 6.48 us -> none  [body(): lax.all_to_all(down_rows, 'tp', split_axis=0, concat_axis=1, tiled=True)]
    convert_element_type x2 -> x0, other arithmetic: 6 us -> none  [the longest x1 3.2 us: body(): up_local = (norm_gain[:, None] * up_train).astype(jnp.bfloat16)]
    all_to_all x1 -> x0, starting transfers between devices: 4.61 us -> none  [body(): lax.all_to_all(down_rows, 'tp', split_axis=0, concat_axis=1, tiled=True)]
    unnamed x11 -> x10, local copies, waits for them, and re-layouts: 13.3 us -> 11.2 us
  transfers between devices with their start and end apart: 6 -> 0, of which waited for: 5 -> 0; matrix products, arithmetic and copies ran while one was open for 8% -> 0% of each run, Pallas kernels for 0% -> 0%
where the time goes in v1:
time: 310 us; the launch traced here: 308 us
  Pallas kernels  295 us (95%)
  local copies, waits for them, and re-layouts  12.8 us (4%)
    pallas_call x1, Pallas kernels, body(): pl.pallas_call(kernel, out_shape=(jax.ShapeDtypeStruct((rows * n_fs, cols...  295 us
    unnamed x10, local copies, waits for them, and re-layouts  11.2 us

profile of v1, /device:TPU:0, one launch (start us, length us, event | category | flops | bytes accessed | tf_op | source)
XLA Modules:
  0.0 308.1 jit_solution(13160587862637865278)
XLA Ops:
  0.6 1.5 copy.9.gain_in
  2.2 294.7 %shard_map.84 = (bf16[2048,1024]{1,0:T(8,128)(2,1)}, bf16[2048,1024]{1,0:T(8,128)(2,1)}, bf16[1024,2048]{1,0:T(8,128)(2,1)}, bf16[64,2048]{1,0:T(8,128)(2,1)}) custom-call(bf16[512,256]{1,0:T(8,128)(2,1)} %tok_in.1, f32[512,1]{1,0:T(8,128)} %copy.9.gain_in, f32[512,1024]{1,0:T(8,128)} %gate_in.1, f32[512,1024]{1,0:T(8,128)} %up_in.1, f32[2048,256]{1,0:T(8,128)} %down_in.1), custom_call_target="tpu_custom_call" | custom-call | tf_op jit(solution)/shard_map/pallas_call | solution.py:324
  296.9 0.0 copy-start.1
  296.9 4.8 %copy.14 = bf16[2048,1024]{1,0:T(8,128)(2,1)} copy(bf16[2048,1024]{1,0:T(8,128)(2,1)} %get-tuple-element.8) | data formatting | bytes 8388608
  301.7 0.0 copy-done.1
  301.7 0.0 copy-start
  301.7 2.1 copy.15
  303.9 1.6 copy-done
  305.4 0.0 copy-start.2
  305.4 2.0 copy.16
  307.4 0.0 copy-done.2
  307.4 0.7 copy.17
Async XLA Ops:
  296.9 4.8 %copy-start.1 = (bf16[2048,1024]{1,0:T(8,128)(2,1)S(1)}, bf16[2048,1024]{1,0:T(8,128)(2,1)}, u32[]{:S(2)}) copy-start(bf16[2048,1024]{1,0:T(8,128)(2,1)} %get-tuple-element.9) | copy-start | bytes 12582916
  301.7 3.7 %copy-start = (bf16[1024,2048]{1,0:T(8,128)(2,1)S(1)}, bf16[1024,2048]{1,0:T(8,128)(2,1)}, u32[]{:S(2)}) copy-start(bf16[1024,2048]{1,0:T(8,128)(2,1)} %get-tuple-element.10) | copy-start | bytes 12582916
  305.4 2.0 copy-start.2

commit v2 on v1

--- a/solution.py
+++ b/solution.py
@@ -14,6 +14,8 @@
 CHUNKS = 4
 X_ORDER = (0, 1, 2, 3)
 Y_ORDER = (2, 3, 0, 1)
+QUARTERS = 4
+LAG = 2
 
 
 def flip(a, k):
@@ -39,7 +41,7 @@
     part = rows // CHUNKS
     w_ins, w_outs = (gate_in, up_in), (gate_out, up_out)
     tall, width = dbuf.shape[1], dbuf.shape[2]
-    half = tall // 2
+    quarter = tall // QUARTERS
     per = n_tp // n_fs
     n_tok = tbuf.shape[1]
     piece_rows = n_tok // n_tp
@@ -96,20 +98,20 @@
             w_copy(w, f, Y_ORDER[step], own_s.at[1, w, Y_ORDER[step]], fy).start()
 
     def dz_copy(c, h):
-        block = pl.ds(h * half, half)
+        block = pl.ds(h * quarter, quarter)
         return remote(dcast.at[c, block], dbuf.at[t, block], dz_s.at[c, h], d_r.at[t, h], f, f * per + c)
 
     for c in range(per):
         load_down[c].wait()
-        for h in range(2):
-            block = pl.ds(h * half, half)
-            dcast[c, block] = d32[pl.ds(c * tall + h * half, half)].astype(BF16)
+        for h in range(QUARTERS):
+            block = pl.ds(h * quarter, quarter)
+            dcast[c, block] = d32[pl.ds(c * tall + h * quarter, quarter)].astype(BF16)
 
         @pl.when(t == f * per + c)
         def _():
             dbuf[t] = dcast[c]
 
-    for h in range(2):
+    for h in range(QUARTERS):
         for c in range(per):
             @pl.when(t != f * per + c)
             def _():
@@ -131,7 +133,7 @@
         if i >= CHUNKS // 2:
             w_copy(w, fy, i, fwd_s.at[w, i], fx).start()
 
-    tile = 256
+    tile = 512
 
     def accumulate(src, first):
         def one(n, _):
@@ -157,11 +159,18 @@
         tok_copy(tbuf.at[piece], piece, 4 + slot, mate).start()
     for k in (1, 3, 5, 7):
         tok_copy(tok_in, flip(t, k), 0, mate).wait_recv()
-    squares = jnp.zeros((n_tok, 1), F32)
-    for p in range(n_tp):
-        wide = tbuf[p].astype(F32)
-        squares = squares + jnp.sum(wide * wide, axis=1, keepdims=True)
-    scale[...] = lax.rsqrt(squares / (n_tp * width) + epsilon)
+    step_rows = n_tok // n_tp
+
+    def norm(i, _):
+        block = pl.ds(i * step_rows, step_rows)
+        squares = 0.0
+        for p in range(n_tp):
+            wide = tbuf[p, block].astype(F32)
+            squares = squares + wide * wide
+        scale[block] = lax.rsqrt(jnp.sum(squares, axis=1, keepdims=True) / (n_tp * width) + epsilon)
+        return 0
+
+    lax.fori_loop(0, n_tp, norm, 0)
     accumulate(f, True)
     for step in range(CHUNKS // 2, CHUNKS):
         for w in range(2):
@@ -179,24 +188,33 @@
     nexts = (to_first, to_second)
 
     def d_copy(piece, h):
-        ref = dbuf.at[piece, pl.ds(h * half, half)]
-        return remote(ref, ref, d_s.at[piece, h], d_r.at[piece, h], nexts[h], t)
-
-    def take(k):
+        ref = dbuf.at[piece, pl.ds(h * quarter, quarter)]
+        return remote(ref, ref, d_s.at[piece, h], d_r.at[piece, h], nexts[h % 2], t)
+
+    def pass_on(k):
         piece = flip(t, k)
-        for h in range(2):
-            @pl.when(jnp.logical_or(jnp.logical_not(is_source), k != 0))
+        for h in range(QUARTERS):
+            @pl.when(ends[h % 2] == 0)
+            def _():
+                if isinstance(k, int) and k == 0:
+                    @pl.when(jnp.logical_not(is_source))
+                    def _():
+                        d_copy(piece, h).wait_recv()
+                else:
+                    d_copy(piece, h).wait_recv()
+                d_copy(piece, h).start()
+
+    def take_last(k):
+        piece = flip(t, k)
+        for h in range(QUARTERS):
+            @pl.when(ends[h % 2] == 1)
             def _():
                 d_copy(piece, h).wait_recv()
 
-            @pl.when(ends[h] == 0)
-            def _():
-                d_copy(piece, h).start()
-
     @pl.when(is_source)
     def _():
-        take(0)
-        take(1)
+        pass_on(0)
+        pass_on(1)
 
     accumulate(fx, False)
     accumulate(fy, False)
@@ -206,6 +224,10 @@
     for w in range(2):
         store_w(w, fd).start()
     accumulate(fd, False)
+
+    @pl.when(jnp.logical_not(is_source))
+    def _():
+        pass_on(0)
 
     def make_hidden(n, _):
         columns = pl.ds(pl.multiple_of(n * tile, tile), tile)
@@ -261,20 +283,29 @@
 
         p_copy(k).start()
 
-    def pair(i, _):
-        for c in range(2):
-            k = 2 * i + c
-
-            @pl.when(jnp.logical_not(jnp.logical_and(is_source, i == 0)))
-            def _():
-                take(k)
-
-            product(k)
-        for c in range(2):
-            finish(2 * i + c)
+    @pl.when(jnp.logical_not(is_source))
+    def _():
+        pass_on(1)
+
+    def step(i, _):
+        made, done = i, i - 2
+
+        @pl.when(i + LAG < n_tp)
+        def _():
+            pass_on(i + LAG)
+
+        @pl.when(made < n_tp)
+        def _():
+            take_last(made)
+            product(made)
+
+        @pl.when(done >= 0)
+        def _():
+            finish(done)
+
         return 0
 
-    lax.fori_loop(0, n_tp // 2, pair, 0)
+    lax.fori_loop(0, n_tp + 2, step, 0)
 
     for k in range(n_tp):
         for dz in range(1, n_z):
@@ -297,7 +328,7 @@
         for src in range(n_fs):
             store_w(w, src).wait()
     for c in range(per):
-        for h in range(2):
+        for h in range(QUARTERS):
             @pl.when(t != f * per + c)
             def _():
                 dz_copy(c, h).wait_send()
@@ -306,8 +337,8 @@
         p_copy(k).wait_send()
         for dz in range(1, n_z):
             z_copy(k, dz, k).wait_send()
-        for h in range(2):
-            @pl.when(ends[h] == 0)
+        for h in range(QUARTERS):
+            @pl.when(ends[h % 2] == 0)
             def _():
                 d_copy(k, h).wait_send()
 
@@ -353,9 +384,9 @@
             dma((2, 2, CHUNKS)),
             dma((2, CHUNKS)),
             dma((2, n_fs, CHUNKS)),
-            dma((n_tp // n_fs, 2)),
-            dma((n_tp, 2)),
-            dma((n_tp, 2)),
+            dma((n_tp // n_fs, QUARTERS)),
+            dma((n_tp, QUARTERS)),
+            dma((n_tp, QUARTERS)),
             dma((2, n_fs)),
             dma((n_tp,)),
             dma((n_tp,)),

time: 310 us -> 160 us (0.52)
  Pallas kernels: 295 us -> 147 us
    pallas_call x1, Pallas kernels: 295 us -> 147 us  [body(): pl.pallas_call(kernel, out_shape=(jax.ShapeDtypeStruct((rows * n_fs, cols...]
where the time goes in v2:
time: 160 us
  Pallas kernels  147 us (92%)
  local copies, waits for them, and re-layouts  12.8 us (8%)
    pallas_call x1, Pallas kernels, body(): pl.pallas_call(kernel, out_shape=(jax.ShapeDtypeStruct((rows * n_fs, cols...  147 us
    unnamed x10, local copies, waits for them, and re-layouts  11.2 us

profile of v2, /device:TPU:0, one launch (start us, length us, event | category | flops | bytes accessed | tf_op | source)
XLA Modules:
  0.0 160.0 jit_solution(2220078508921324499)
XLA Ops:
  0.6 1.5 copy.9.gain_in
  2.2 146.6 %shard_map.84 = (bf16[2048,1024]{1,0:T(8,128)(2,1)}, bf16[2048,1024]{1,0:T(8,128)(2,1)}, bf16[1024,2048]{1,0:T(8,128)(2,1)}, bf16[64,2048]{1,0:T(8,128)(2,1)}) custom-call(bf16[512,256]{1,0:T(8,128)(2,1)} %tok_in.1, f32[512,1]{1,0:T(8,128)} %copy.9.gain_in, f32[512,1024]{1,0:T(8,128)} %gate_in.1, f32[512,1024]{1,0:T(8,128)} %up_in.1, f32[2048,256]{1,0:T(8,128)} %down_in.1), custom_call_target="tpu_custom_call" | custom-call | tf_op jit(solution)/shard_map/pallas_call | solution.py:355
  148.8 0.0 copy-start.1
  148.8 4.8 %copy.14 = bf16[2048,1024]{1,0:T(8,128)(2,1)} copy(bf16[2048,1024]{1,0:T(8,128)(2,1)} %get-tuple-element.8) | data formatting | bytes 8388608
  153.6 0.0 copy-done.1
  153.6 0.0 copy-start
  153.6 2.1 %copy.15 = bf16[2048,1024]{1,0:T(8,128)(2,1)} copy(bf16[2048,1024]{1,0:T(8,128)(2,1)S(1)} %copy-done.1) | data formatting | bytes 8388608
  155.7 1.6 copy-done
  157.3 0.0 copy-start.2
  157.3 2.0 %copy.16 = bf16[1024,2048]{1,0:T(8,128)(2,1)} copy(bf16[1024,2048]{1,0:T(8,128)(2,1)S(1)} %copy-done) | data formatting | bytes 8388608
  159.3 0.0 copy-done.2
  159.3 0.7 copy.17
Async XLA Ops:
  148.8 4.8 %copy-start.1 = (bf16[2048,1024]{1,0:T(8,128)(2,1)S(1)}, bf16[2048,1024]{1,0:T(8,128)(2,1)}, u32[]{:S(2)}) copy-start(bf16[2048,1024]{1,0:T(8,128)(2,1)} %get-tuple-element.9) | copy-start | bytes 12582916
  153.6 3.7 %copy-start = (bf16[1024,2048]{1,0:T(8,128)(2,1)S(1)}, bf16[1024,2048]{1,0:T(8,128)(2,1)}, u32[]{:S(2)}) copy-start(bf16[1024,2048]{1,0:T(8,128)(2,1)} %get-tuple-element.10) | copy-start | bytes 12582916
  157.3 2.0 %copy-start.2 = (bf16[64,2048]{1,0:T(8,128)(2,1)S(1)}, bf16[64,2048]{1,0:T(8,128)(2,1)}, u32[]{:S(2)}) copy-start(bf16[64,2048]{1,0:T(8,128)(2,1)} %get-tuple-element.11) | copy-start | bytes 786436
